TPU v7x, 32 devices: a whole 2x2x4 slice. The times are simulated.
32 devices in a mesh: sp: 4 (over z), dp: 8 (over y, x, core).
Axes of the slice: x: 2, y: 2, z: 4, core: 2. Of those that a mesh axis runs over, the one named last changes fastest.
Arguments:
- probe_vectors: bfloat16 [4096, 1024], P(('dp', 'sp')), may hold values from -6 to 6
- address_vectors: bfloat16 [4096, 1024], P(('dp', 'sp')), may hold values from -6 to 6
- content_vectors: bfloat16 [4096, 2048], P(('dp', 'sp')), may hold values from -6 to 6
- adjoint_of_result: bfloat16 [4096, 2048], P(('dp', 'sp')), may hold values from -0.5 to 0.5
- compact_factor: bfloat16 [4096, 64], P(('dp', 'sp')), may hold values from -7.5 to 7.5
- latent_to_damping_map: bfloat16 [64, 1024], replicated, may hold values from -0.75 to 0.75
- damping_shift_term: float32 [1024], replicated
- surplus_damping: bfloat16 [4096, 16], P(('dp', 'sp')), may hold values from -0.7 to 0
Outputs:
- query_grad: bfloat16 [4096, 1024], P(('dp', 'sp'))
- key_grad: bfloat16 [4096, 1024], P(('dp', 'sp'))
- value_grad: bfloat16 [4096, 2048], P(('dp', 'sp'))
- latent_grad: bfloat16 [4096, 64], P(('dp', 'sp'))
- weight_grad: float32 [64, 1024], replicated
All inputs are finite; a program needn't handle non-finite values.
Results may differ from a plain program's by a relative error of at most 0.005.
Values may be sent and summed in bfloat16 or wider, within the bound.
No kernel may reach another device: no remote copies, remote signals or barrier semaphores. Data moves between devices by JAX's collectives and lax.ppermute only.
A program may use at most 64 MiB of HBM per device.

v0:
```python
import jax
import jax.numpy as jnp
from jax import lax
from jax.sharding import PartitionSpec as P

KEY_CHANNELS = 64
VALUE_DIM = 128
BLOCK = 64
gate_norm = 16.0
highest = lax.Precision.HIGHEST


def carry_states(block_total, increments):
    log_totals = block_total[:, :, 0, :]
    running = jnp.cumsum(log_totals, axis=1)
    before = running - log_totals
    blocks = log_totals.shape[1]
    order = jnp.arange(blocks, dtype=jnp.int32)
    earlier_mask = (order[None, :] < order[:, None])[None, :, :, None]
    exponent = before[:, :, None, :] - running[:, None, :, :]
    exponent = jnp.where(earlier_mask, exponent, jnp.zeros_like(exponent))
    weights = jnp.where(earlier_mask, jnp.exp(exponent), jnp.zeros_like(exponent))
    return jnp.einsum("hnmk,mhkv->nhkv", weights, increments, precision=highest)


def gla_forward(probe_vectors, address_vectors, content_vectors, logarithm_decay):
    head_count, seq_len, key_width = probe_vectors.shape
    value_width = content_vectors.shape[2]
    blocks = seq_len // BLOCK

    def blocked(tensor):
        return tensor.reshape(head_count, blocks, BLOCK, tensor.shape[2])

    cumulative = jnp.cumsum(blocked(logarithm_decay), axis=2)
    block_total = cumulative[:, :, BLOCK - 1 :, :]
    keys_block = blocked(address_vectors)
    query_decayed = blocked(probe_vectors) * key_width ** (-0.5) * jnp.exp(cumulative)
    key_inverse = keys_block * jnp.exp(-cumulative)
    key_to_end = keys_block * jnp.exp(block_total - cumulative)
    value_block = blocked(content_vectors)
    scores = jnp.einsum("hnik,hnjk->hnij", query_decayed, key_inverse, precision=highest)
    positions = jnp.arange(BLOCK, dtype=jnp.int32)
    causal = positions[:, None] >= positions[None, :]
    scores = jnp.where(causal, scores, jnp.zeros_like(scores))
    within_block = jnp.einsum("hnij,hnjv->hniv", scores, value_block, precision=highest)
    increments = jnp.einsum("hnjk,hnjv->nhkv", key_to_end, value_block, precision=highest)
    earlier = carry_states(block_total, increments)
    carried = jnp.einsum("hnik,nhkv->hniv", query_decayed, earlier, precision=highest)
    return (within_block + carried).reshape(head_count, seq_len, value_width)


def split_into_heads(tensor, width):
    return tensor.astype(jnp.float32).reshape(tensor.shape[0], -1, width).transpose(1, 0, 2)


def to_rows(tensor):
    return tensor.transpose(1, 0, 2).reshape(tensor.shape[1], tensor.shape[0] * tensor.shape[2])


def on_device(
    probe_vectors,
    address_vectors,
    content_vectors,
    adjoint_of_result,
    compact_factor,
    latent_to_damping_map,
    damping_shift_term,
    surplus_damping,
):
    query_per_head, key_per_head, value_per_head, upstream_heads, spike_heads = (
        lax.all_to_all(probe_vectors, "sp", split_axis=1, concat_axis=0, tiled=True),
        lax.all_to_all(address_vectors, "sp", split_axis=1, concat_axis=0, tiled=True),
        lax.all_to_all(content_vectors, "sp", split_axis=1, concat_axis=0, tiled=True),
        lax.all_to_all(adjoint_of_result, "sp", split_axis=1, concat_axis=0, tiled=True),
        lax.all_to_all(surplus_damping, "sp", split_axis=1, concat_axis=0, tiled=True),
    )
    local_width = query_per_head.shape[1]
    hidden_code_rows = lax.all_gather(compact_factor, "sp", axis=0, tiled=True)
    column_start = lax.axis_index("sp") * local_width
    weight_local = lax.dynamic_slice_in_dim(latent_to_damping_map, column_start, local_width, 1)
    bias_local = lax.dynamic_slice_in_dim(damping_shift_term, column_start, local_width, 0)
    gate_logit = (
        jnp.dot(hidden_code_rows, weight_local, preferred_element_type=jnp.float32) + bias_local
    )
    forget_rate_rows = jax.nn.log_sigmoid(gate_logit) / gate_norm
    logarithm_decay = (
        split_into_heads(forget_rate_rows, KEY_CHANNELS)
        + spike_heads.astype(jnp.float32).T[:, :, None]
    )
    _, pullback = jax.vjp(
        gla_forward,
        split_into_heads(query_per_head, KEY_CHANNELS),
        split_into_heads(key_per_head, KEY_CHANNELS),
        split_into_heads(value_per_head, VALUE_DIM),
        logarithm_decay,
    )
    grad_query, grad_key, grad_value, grad_decay = pullback(
        split_into_heads(upstream_heads, VALUE_DIM)
    )
    query_grad, key_grad, value_grad = (
        lax.all_to_all(
            to_rows(grad_query).astype(jnp.bfloat16), "sp", split_axis=0, concat_axis=1, tiled=True
        ),
        lax.all_to_all(
            to_rows(grad_key).astype(jnp.bfloat16), "sp", split_axis=0, concat_axis=1, tiled=True
        ),
        lax.all_to_all(
            to_rows(grad_value).astype(jnp.bfloat16), "sp", split_axis=0, concat_axis=1, tiled=True
        ),
    )
    decay_rows = to_rows(grad_decay)
    gate_grad = (decay_rows * jax.nn.sigmoid(-gate_logit) / gate_norm).astype(jnp.bfloat16)
    partial_latent = jnp.einsum(
        "sc,rc->sr", gate_grad, weight_local, preferred_element_type=jnp.float32
    )
    latent_grad = lax.psum_scatter(partial_latent, "sp", scatter_dimension=0, tiled=True).astype(
        jnp.bfloat16
    )
    local_weight = jnp.einsum(
        "sr,sc->rc", hidden_code_rows, gate_grad, preferred_element_type=jnp.float32
    )
    summed = lax.psum(local_weight, "dp")
    weight_grad = lax.all_gather(summed, "sp", axis=1, tiled=True)
    return (query_grad, key_grad, value_grad, latent_grad, weight_grad)


def solution(mesh):
    return jax.shard_map(
        on_device,
        mesh=mesh,
        in_specs=(
            P(("dp", "sp"), None),
            P(("dp", "sp"), None),
            P(("dp", "sp"), None),
            P(("dp", "sp"), None),
            P(("dp", "sp"), None),
            P(),
            P(),
            P(("dp", "sp"), None),
        ),
        out_specs=(
            P(("dp", "sp"), None),
            P(("dp", "sp"), None),
            P(("dp", "sp"), None),
            P(("dp", "sp"), None),
            P(),
        ),
        check_vma=False,
    )
```

profile of v0, /device:TPU:0, one launch (start us, length us, event | category | flops | bytes accessed | tf_op | source)
XLA Modules:
  0.0 277.0 jit_solution(3052615414394250195)
XLA Ops:
  8.0 6.5 %all-to-all-start.1 = ((bf16[128,4,4]{0,2,1:T(4,128)(2,1)}), bf16[128,4,4]{0,2,1:T(4,128)(2,1)S(1)}, u32[]{:S(2)}, u32[]{:S(2)}) async-start(bf16[128,4,4]{0,2,1:T(4,128)(2,1)} %bitcast.169), calls=%async_computation.1 | async-start | bytes 8192 | tf_op jit(solution)/shard_map/all_to_all | solution.py:75
  14.5 1.8 copy.214
  16.3 3.8 %all-to-all-done.1 = bf16[128,4,4]{0,2,1:T(4,128)(2,1)S(1)} async-done(((bf16[128,4,4]{0,2,1:T(4,128)(2,1)}), bf16[128,4,4]{0,2,1:T(4,128)(2,1)S(1)}, u32[]{:S(2)}, u32[]{:S(2)}) %all-to-all-start.1) | async-done | bytes 4128 | tf_op jit(solution)/shard_map/all_to_all | solution.py:75
  20.1 3.5 %all-to-all-start.5 = ((bf16[128,4,256]{0,2,1:T(8,128)(2,1)}), bf16[128,4,256]{0,2,1:T(8,128)(2,1)S(1)}, u32[]{:S(2)}, u32[]{:S(2)}) async-start(bf16[128,4,256]{0,2,1:T(8,128)(2,1)} %bitcast.24), calls=%async_computation.5 | async-start | bytes 524288 | tf_op jit(solution)/shard_map/all_to_all | solution.py:71
  24.5 7.0 %all-to-all-done.5 = bf16[128,4,256]{0,2,1:T(8,128)(2,1)S(1)} async-done(((bf16[128,4,256]{0,2,1:T(8,128)(2,1)}), bf16[128,4,256]{0,2,1:T(8,128)(2,1)S(1)}, u32[]{:S(2)}, u32[]{:S(2)}) %all-to-all-start.5) | async-done | bytes 262176 | tf_op jit(solution)/shard_map/all_to_all | solution.py:71
  31.5 3.4 %all-to-all-start = ((bf16[128,4,256]{0,2,1:T(8,128)(2,1)}), bf16[128,4,256]{0,2,1:T(8,128)(2,1)S(1)}, u32[]{:S(2)}, u32[]{:S(2)}) async-start(bf16[128,4,256]{0,2,1:T(8,128)(2,1)} %bitcast), calls=%async_computation | async-start | bytes 524288 | tf_op jit(solution)/shard_map/all_to_all | solution.py:72
  36.6 12.5 %all_gather.6 = bf16[512,64]{0,1:T(8,128)(2,1)S(1)} all-gather(bf16[128,64]{0,1:T(8,128)(2,1)S(1)} %copy-done.31), channel_id=1, replica_groups=mesh['sp'=4,'dp'=8] {'sp'}, dimensions={0}, use_global_device_ids=true | all-gather | bytes 81920 | tf_op jit(solution)/shard_map/all_gather | solution.py:78
  49.7 1.3 fusion.20
  51.7 4.1 %all-to-all-start.3 = ((bf16[128,4,512]{2,0,1:T(8,128)(2,1)}), bf16[128,4,512]{2,0,1:T(8,128)(2,1)}, u32[]{:S(2)}, u32[]{:S(2)}) async-start(bf16[128,4,512]{2,0,1:T(8,128)(2,1)} %bitcast.143), calls=%async_computation.3 | async-start | bytes 1048576 | tf_op jit(solution)/shard_map/all_to_all | solution.py:74
  56.4 0.9 copy.312
  58.0 25.9 %fusion.46 = f32[4,8,64,64]{3,1,2,0:T(8,128)S(1)} fusion(f32[4,8,64,64]{3,1,2,0:T(8,128)S(1)} %copy.194), kind=kOutput, calls=%fused_computation.84 | output fusion | flops 8257536 | bytes 1048576 | tf_op jit(solution)/shard_map/jvp(jit(cumsum))/reduce_window_sum | solution.py:34
  83.9 5.1 %all-to-all-start.2 = ((bf16[128,4,512]{2,0,1:T(8,128)(2,1)}), bf16[128,4,512]{2,0,1:T(8,128)(2,1)}, u32[]{:S(2)}, u32[]{:S(2)}) async-start(bf16[128,4,512]{2,0,1:T(8,128)(2,1)} %bitcast.144), calls=%async_computation.2 | async-start | bytes 1048576 | tf_op jit(solution)/shard_map/all_to_all | solution.py:73
  92.8 1.0 reshape.170
  93.8 1.2 reshape.166
  95.1 2.0 reshape.161
  97.0 1.9 copy.205
  99.4 2.0 reshape.159
  101.3 1.2 copy.198
  102.6 0.9 convolution_bitcast_fusion.3
  103.7 2.9 %convolution_bitcast_fusion = f32[8,4,64,128]{3,0,2,1:T(8,128)S(1)} fusion(f32[4,64,128,8]{2,1,3,0:T(8,128)S(1)} %convolution_bitcast_fusion.3, f32[4,8,64]{1,2,0:T(8,128)S(1)} %copy-done.23, f32[4,8,64]{1,2,0:T(8,128)S(1)} %copy-done.24, pred[8,8]{1,0:T(8,128)(4,1)S(1)} %copy-done.32), kind=kOutput, calls=%fused_computation.4 | convolution fusion | flops 25214976 | bytes 2113600 | tf_op jit(solution)/shard_map/transpose(jvp(hnmk,mhkv->nhkv))/dot_general | solution.py:23
  106.6 2.8 %fusion.18 = (f32[4,8,64]{2,1,0:T(8,128)}, f32[4,8,64,64]{2,3,1,0:T(8,128)S(1)}, f32[4,8,64,64]{2,3,1,0:T(8,128)}) fusion(f32[4,8,64,64]{2,3,1,0:T(8,128)S(1)} %copy.195, f32[4,8,64,64]{2,1,3,0:T(8,128)S(1)} %reshape.166, f32[4,8,64]{2,1,0:T(8,128)S(1)} %slice_bitcast_fusion, bf16[4,8,64,128]{3,2,1,0:T(8,128)(2,1)S(1)} %bitcast.150, ...), kind=kOutput, calls=%fused_computation.40 | convolution fusion | flops 201979904 | bytes 3686400 | tf_op jit(solution)/shard_map/transpose(jvp(hnjk,hnjv->nhkv))/dot_general | solution.py:46
  110.4 2.5 convolution_bitcast_fusion.1
  112.9 4.3 %fusion.45 = (f32[4,8,64]{1,2,0:T(8,128)}, f32[4,8,64]{1,2,0:T(8,128)}) fusion(f32[4,8,64]{1,2,0:T(8,128)S(1)} %copy-done.23, f32[4,8,64]{1,2,0:T(8,128)S(1)} %copy-done.24, f32[8,4,64,128]{3,2,1,0:T(8,128)S(1)} %fusion.6, f32[4,64,128,8]{2,1,3,0:T(8,128)S(1)} %convolution_bitcast_fusion.3, pred[8,8]{1,0:T(8,128)(4,1)S(1)} %copy-done.32), kind=kOutput, calls=%fused_computation.83 | convolution fusion | flops 25276416 | bytes 2129984 | tf_op jit(solution)/shard_map/transpose(jvp(hnmk,mhkv->nhkv))/dot_general | solution.py:23
  117.3 2.0 convolution_bitcast_fusion.4
  120.9 1.4 copy.243
  122.2 1.4 copy.244
  123.6 1.4 copy.245
  125.1 1.6 convolution_select_fusion
  126.7 1.3 fusion.44
  128.6 1.5 fusion.3
  130.1 3.7 %pad_add_fusion = (f32[4,8,64,64]{2,3,1,0:T(8,128)}, bf16[4,8,64,64]{2,3,1,0:T(8,128)(2,1)}, bf16[4,8,64,64]{2,3,1,0:T(8,128)(2,1)S(1)}) fusion(f32[4,8,1,64]{2,3,1,0:T(8,128)S(1)} %fusion.3, f32[4,8,64,64]{2,3,1,0:T(8,128)S(1)} %fusion.44, f32[4,8,64,64]{2,1,3,0:T(8,128)S(1)} %mul.72, f32[4,8,64,64]{2,3,1,0:T(8,128)S(1)} %copy.195, ...), kind=kOutput, calls=%fused_computation.22 | convolution fusion | flops 103677952 | bytes 4734976 | tf_op jit(solution)/shard_map/transpose(jvp(hnik,hnjk->hnij))/dot_general | solution.py:41
  133.8 1.1 copy.212
  134.9 1.4 convert_element_type.73
  137.1 1.7 copy.213
  138.8 4.8 %all-to-all-start.4 = ((bf16[4,128,256]{1,2,0:T(8,128)(2,1)}), bf16[4,128,256]{1,2,0:T(8,128)(2,1)S(1)}, u32[]{:S(2)}, u32[]{:S(2)}) async-start(bf16[4,128,256]{1,2,0:T(8,128)(2,1)} %copy.213), calls=%async_computation.4 | async-start | bytes 524288 | tf_op jit(solution)/shard_map/all_to_all | solution.py:101
  143.6 3.1 %convolution_select_fusion.2 = f32[4,8,64,64]{3,2,1,0:T(8,128)} fusion(pred[64,64]{1,0:T(8,128)(4,1)S(1)} %copy-done.28, f32[4,8,64,64]{2,1,3,0:T(8,128)S(1)} %reshape.166, f32[4,8,64,64]{2,3,1,0:T(8,128)S(1)} %copy.195, f32[4,8,64,64]{2,1,3,0:T(8,128)S(1)} %mul.72), kind=kOutput, calls=%fused_computation.11 | convolution fusion | flops 101187584 | bytes 2101248 | tf_op jit(solution)/shard_map/jvp(hnik,hnjk->hnij)/dot_general | solution.py:41
  148.3 3.2 %fusion.11 = f32[4,8,64,128]{3,2,1,0:T(8,128)S(1)} fusion(f32[4,8,64,64]{2,3,1,0:T(8,128)S(1)} %copy-done.4, f32[8,4,64,128]{3,0,2,1:T(8,128)} %copy-done.9), kind=kOutput, calls=%fused_computation.30 | convolution fusion | flops 201326592 | bytes 2621440 | tf_op jit(solution)/shard_map/transpose(jvp(hnjk,hnjv->nhkv))/dot_general | solution.py:46
  151.5 5.2 %all-to-all-start.6 = ((bf16[4,128,256]{1,2,0:T(8,128)(2,1)}), bf16[4,128,256]{1,2,0:T(8,128)(2,1)S(1)}, u32[]{:S(2)}, u32[]{:S(2)}) async-start(bf16[4,128,256]{1,2,0:T(8,128)(2,1)} %copy.226), calls=%async_computation.6 | async-start | bytes 524288 | tf_op jit(solution)/shard_map/all_to_all | solution.py:104
  156.7 1.0 fusion.4
  158.2 1.0 convert_element_type.84
  159.6 25.8 %fusion.47 = f32[4,8,64,64]{3,1,2,0:T(8,128)S(1)} fusion(f32[4,8,64,64]{3,1,2,0:T(8,128)S(1)} %copy.246), kind=kOutput, calls=%fused_computation.85 | output fusion | flops 8257536 | bytes 1048576 | tf_op jit(solution)/shard_map/transpose(jvp(jit(cumsum)))/reduce_window_sum | solution.py:34
  186.1 5.2 %all-to-all-start.7 = ((bf16[4,128,512]{2,1,0:T(8,128)(2,1)}), bf16[4,128,512]{2,1,0:T(8,128)(2,1)S(1)}, u32[]{:S(2)}, u32[]{:S(2)}) async-start(bf16[4,128,512]{2,1,0:T(8,128)(2,1)} %convert_element_type.84), calls=%async_computation.7 | async-start | bytes 1048576 | tf_op jit(solution)/shard_map/all_to_all | solution.py:107
  193.9 56.5 %all-reduce.3.cloned.1.call-done = f32[64,256]{1,0:T(8,128)} async-done(((f32[64,256]{1,0:T(8,128)}), f32[64,256]{1,0:T(8,128)}) %all-reduce.3.cloned.1.call-update) | async-done | bytes 65552 | tf_op jit(solution)/shard_map/psum | solution.py:122
  250.4 14.1 %all_gather.7 = f32[64,1024]{1,0:T(8,128)S(1)} all-gather(f32[64,256]{1,0:T(8,128)} %all-reduce.3.cloned.1.call-done), channel_id=1, replica_groups=mesh['sp'=4,'dp'=8] {'sp'}, dimensions={1}, use_global_device_ids=true | all-gather | bytes 327680 | tf_op jit(solution)/shard_map/all_gather | solution.py:123
  264.5 1.4 convert_element_type.86
  265.9 0.8 copy.248
  266.7 0.8 copy.249
  267.9 1.0 copy.250
  (116 shorter events, 20.1 us)
Async XLA Ops:
  8.0 41.7 %copy-start = (bf16[64,1024]{1,0:T(8,128)(2,1)S(1)}, bf16[64,1024]{1,0:T(8,128)(2,1)}, u32[]{:S(2)}) copy-start(bf16[64,1024]{1,0:T(8,128)(2,1)} %param.13) | copy-start | bytes 393220
  8.0 12.1 %all-to-all-start.1 = ((bf16[128,4,4]{0,2,1:T(4,128)(2,1)}), bf16[128,4,4]{0,2,1:T(4,128)(2,1)S(1)}, u32[]{:S(2)}, u32[]{:S(2)}) async-start(bf16[128,4,4]{0,2,1:T(4,128)(2,1)} %bitcast.169), calls=%async_computation.1 | async-start | bytes 8192 | tf_op jit(solution)/shard_map/all_to_all | solution.py:75
  20.1 3.6 %copy-start.20 = (bf16[128,1024]{1,0:T(8,128)(2,1)S(1)}, bf16[128,1024]{1,0:T(8,128)(2,1)}, u32[]{:S(2)}) copy-start(bf16[128,1024]{1,0:T(8,128)(2,1)} %param.9) | copy-start | bytes 786436
  20.1 11.4 %all-to-all-start.5 = ((bf16[128,4,256]{0,2,1:T(8,128)(2,1)}), bf16[128,4,256]{0,2,1:T(8,128)(2,1)S(1)}, u32[]{:S(2)}, u32[]{:S(2)}) async-start(bf16[128,4,256]{0,2,1:T(8,128)(2,1)} %bitcast.24), calls=%async_computation.5 | async-start | bytes 524288 | tf_op jit(solution)/shard_map/all_to_all | solution.py:71
  23.6 11.3 %copy-start.17 = (bf16[128,2048]{1,0:T(8,128)(2,1)S(1)}, bf16[128,2048]{1,0:T(8,128)(2,1)}, u32[]{:S(2)}) copy-start(bf16[128,2048]{1,0:T(8,128)(2,1)} %param.11) | copy-start | bytes 1572868
  31.5 19.5 %all-to-all-start = ((bf16[128,4,256]{0,2,1:T(8,128)(2,1)}), bf16[128,4,256]{0,2,1:T(8,128)(2,1)S(1)}, u32[]{:S(2)}, u32[]{:S(2)}) async-start(bf16[128,4,256]{0,2,1:T(8,128)(2,1)} %bitcast), calls=%async_computation | async-start | bytes 524288 | tf_op jit(solution)/shard_map/all_to_all | solution.py:72
  35.0 1.6 copy-start.31
  49.0 1.9 copy-start.21
  51.0 0.7 copy-start.15
  51.0 5.4 %copy-start.18 = (bf16[128,2048]{1,0:T(8,128)(2,1)S(1)}, bf16[128,2048]{1,0:T(8,128)(2,1)}, u32[]{:S(2)}) copy-start(bf16[128,2048]{1,0:T(8,128)(2,1)} %param.10) | copy-start | bytes 1572868
  51.7 32.2 %all-to-all-start.3 = ((bf16[128,4,512]{2,0,1:T(8,128)(2,1)}), bf16[128,4,512]{2,0,1:T(8,128)(2,1)}, u32[]{:S(2)}, u32[]{:S(2)}) async-start(bf16[128,4,512]{2,0,1:T(8,128)(2,1)} %bitcast.143), calls=%async_computation.3 | async-start | bytes 1048576 | tf_op jit(solution)/shard_map/all_to_all | solution.py:74
  83.9 15.5 %all-to-all-start.2 = ((bf16[128,4,512]{2,0,1:T(8,128)(2,1)}), bf16[128,4,512]{2,0,1:T(8,128)(2,1)}, u32[]{:S(2)}, u32[]{:S(2)}) async-start(bf16[128,4,512]{2,0,1:T(8,128)(2,1)} %bitcast.144), calls=%async_computation.2 | async-start | bytes 1048576 | tf_op jit(solution)/shard_map/all_to_all | solution.py:73
  91.5 1.0 copy-start.16
  101.3 1.2 copy-start.1
  102.5 7.0 %copy-start.5 = (bf16[4,512,128]{2,1,0:T(8,128)(2,1)}, bf16[4,512,128]{2,1,0:T(8,128)(2,1)S(1)}, u32[]{:S(2)}) copy-start(bf16[4,512,128]{2,1,0:T(8,128)(2,1)S(1)} %copy.198) | copy-start | bytes 1572868
  102.5 1.1 copy-start.23
  102.5 1.1 copy-start.24
  102.5 1.1 copy-start.32
  106.6 2.9 %copy-start.9 = (f32[8,4,64,128]{3,0,2,1:T(8,128)}, f32[8,4,64,128]{3,0,2,1:T(8,128)S(1)}, u32[]{:S(2)}) copy-start(f32[8,4,64,128]{3,0,2,1:T(8,128)S(1)} %convolution_bitcast_fusion) | copy-start | bytes 3145732
  109.5 1.0 copy-start.3
  117.3 2.0 copy-start.26
  119.2 0.9 copy-start.25
  120.1 0.7 copy-start.30
  122.2 1.4 copy-start.29
  123.6 1.4 copy-start.27
  126.7 1.3 copy-start.11
  126.7 1.5 copy-start.12
  126.7 1.8 copy-start.13
  128.5 1.5 copy-start.8
  128.5 1.5 copy-start.10
  138.8 4.8 %copy-start.28 = (pred[64,64]{1,0:T(8,128)(4,1)S(1)}, pred[64,64]{1,0:T(8,128)(4,1)}, u32[]{:S(2)}) copy-start(pred[64,64]{1,0:T(8,128)(4,1)} %iota_compare_fusion) | copy-start | bytes 12292
  138.8 12.7 %all-to-all-start.4 = ((bf16[4,128,256]{1,2,0:T(8,128)(2,1)}), bf16[4,128,256]{1,2,0:T(8,128)(2,1)S(1)}, u32[]{:S(2)}, u32[]{:S(2)}) async-start(bf16[4,128,256]{1,2,0:T(8,128)(2,1)} %copy.213), calls=%async_computation.4 | async-start | bytes 524288 | tf_op jit(solution)/shard_map/all_to_all | solution.py:101
  143.6 3.1 %copy-start.14 = (bf16[4,8,64,64]{2,3,1,0:T(8,128)(2,1)S(1)}, bf16[4,8,64,64]{2,3,1,0:T(8,128)(2,1)}, u32[]{:S(2)}) copy-start(bf16[4,8,64,64]{2,3,1,0:T(8,128)(2,1)} %get-tuple-element.23) | copy-start | bytes 786436
  147.1 1.2 copy-start.4
  148.3 8.4 %copy-start.6 = (f32[4,8,64,64]{3,2,1,0:T(8,128)S(1)}, f32[4,8,64,64]{3,2,1,0:T(8,128)}, u32[]{:S(2)}) copy-start(f32[4,8,64,64]{3,2,1,0:T(8,128)} %convolution_select_fusion.2) | copy-start | bytes 1572868
  151.5 5.3 %copy-start.2 = (bf16[4,512,128]{2,1,0:T(8,128)(2,1)S(1)}, bf16[4,512,128]{2,1,0:T(8,128)(2,1)}, u32[]{:S(2)}) copy-start(bf16[4,512,128]{2,1,0:T(8,128)(2,1)} %copy.205) | copy-start | bytes 1572868
  151.5 34.6 %all-to-all-start.6 = ((bf16[4,128,256]{1,2,0:T(8,128)(2,1)}), bf16[4,128,256]{1,2,0:T(8,128)(2,1)S(1)}, u32[]{:S(2)}, u32[]{:S(2)}) async-start(bf16[4,128,256]{1,2,0:T(8,128)(2,1)} %copy.226), calls=%async_computation.6 | async-start | bytes 524288 | tf_op jit(solution)/shard_map/all_to_all | solution.py:104
  157.7 1.4 copy-start.7
  186.1 5.3 %copy-start.19 = (f32[256,512]{1,0:T(8,128)S(1)}, f32[256,512]{1,0:T(8,128)}, u32[]{:S(2)}) copy-start(f32[256,512]{1,0:T(8,128)} %get-tuple-element.30) | copy-start | bytes 1572868
  186.1 81.5 %all-to-all-start.7 = ((bf16[4,128,512]{2,1,0:T(8,128)(2,1)}), bf16[4,128,512]{2,1,0:T(8,128)(2,1)S(1)}, u32[]{:S(2)}, u32[]{:S(2)}) async-start(bf16[4,128,512]{2,1,0:T(8,128)(2,1)} %convert_element_type.84), calls=%async_computation.7 | async-start | bytes 1048576 | tf_op jit(solution)/shard_map/all_to_all | solution.py:107
  191.3 59.1 %all-reduce.3.cloned.1.call-start = ((), (), s32[]{:S(2)}) async-start(), calls=%async_computation.10 | async-start | bytes 131072 | tf_op jit(solution)/shard_map/psum | solution.py:122
  191.3 0.8 copy-start.22
  193.0 71.5 %reduce-scatter.2.cloned.1.call-start = ((), (), s32[]{:S(2)}) async-start(), calls=%async_computation.9 | async-start | bytes 163840 | tf_op jit(solution)/shard_map/reduce_scatter | solution.py:116
Sparse Core Ops, SparseCore 0:
  195.7 54.6 all-reduce.2
Sparse Core Ops, SparseCore 1:
  196.3 20.9 reduce-scatter.1
where the time goes:
time: 279 us; the launch traced here: 277 us
  waiting for transfers between devices  67.7 us (24%)
  other arithmetic  56 us (20%)
  local copies, waits for them, and re-layouts  39.8 us (14%)
  starting transfers between devices  38 us (14%)
  matrix products  32.9 us (12%)
  blocking collectives  26.6 us (10%)
  between operations  15.9 us (6%)
    psum x1, waiting for transfers between devices, on_device(): summed = lax.psum(local_weight, 'dp')  56.5 us
    another operation x2, other arithmetic, gla_forward(): cumulative = jnp.cumsum(blocked(logarithm_decay), axis=2)  51.6 us
    all_gather x1, blocking collectives, on_device(): weight_grad = lax.all_gather(summed, 'sp', axis=1, tiled=True)  14.1 us
    all_gather x1, blocking collectives, on_device(): hidden_code_rows = lax.all_gather(compact_factor, 'sp', axis=0, tiled=True)  12.5 us
    unnamed x72, local copies, waits for them, and re-layouts  10.3 us
    dot_general x3, matrix products, carry_states(): return jnp.einsum('hnmk,mhkv->nhkv', weights, increments, precision=highest)  9.75 us
    dot_general x3, matrix products, gla_forward(): jnp.einsum('hnik,hnjk->hnij', query_decayed, key_inverse, precision=highest)  8.12 us
    all_to_all x1, waiting for transfers between devices, on_device(): lax.all_to_all(probe_vectors, 'sp', split_axis=1, concat_axis=0, tiled=True)  7.02 us
  transfers between devices with their start and end apart: 10, of which 4 were waited for; matrix products, arithmetic and copies ran while one was open for 31% of the time, Pallas kernels for 0%

commit v1 on v0

--- a/solution.py
+++ b/solution.py
@@ -8,6 +8,15 @@
 BLOCK = 64
 gate_norm = 16.0
 highest = lax.Precision.HIGHEST
+
+
+def add_in_pairs(value, name):
+    count = lax.axis_size(name)
+    total, far = (value, 1)
+    while far < count:
+        total = total + lax.ppermute(total, name, [(i, i ^ far) for i in range(count)])
+        far = 2 * far
+    return total
 
 
 def carry_states(block_total, increments):
@@ -119,7 +128,7 @@
     local_weight = jnp.einsum(
         "sr,sc->rc", hidden_code_rows, gate_grad, preferred_element_type=jnp.float32
     )
-    summed = lax.psum(local_weight, "dp")
+    summed = add_in_pairs(local_weight, "dp")
     weight_grad = lax.all_gather(summed, "sp", axis=1, tiled=True)
     return (query_grad, key_grad, value_grad, latent_grad, weight_grad)
 

time: 279 us -> 211 us (0.76)
  waiting for transfers between devices: 67.7 us -> 17.1 us
  other arithmetic: 56 us -> 32.6 us
  local copies, waits for them, and re-layouts: 39.8 us -> 45.5 us
  starting transfers between devices: 38 us -> 41 us
    psum x1 -> x0, waiting for transfers between devices: 56.5 us -> none  [on_device(): summed = lax.psum(local_weight, 'dp')]
    another operation x2, other arithmetic: 51.6 us -> 28.2 us  [gla_forward(): cumulative = jnp.cumsum(blocked(logarithm_decay), axis=2)]
    ppermute x0 -> x3, waiting for transfers between devices: none -> 5.9 us  [add_in_pairs(): lax.ppermute(total, name, [(i, i ^ far) for i in range(count)])]
    ppermute x0 -> x3, starting transfers between devices: none -> 3.22 us  [add_in_pairs(): lax.ppermute(total, name, [(i, i ^ far) for i in range(count)])]
  transfers between devices with their start and end apart: 10 -> 12, of which waited for: 4 -> 6; matrix products, arithmetic and copies ran while one was open for 31% -> 31% of each run, Pallas kernels for 0% -> 0%
where the time goes in v1:
time: 211 us; the launch traced here: 209 us
  local copies, waits for them, and re-layouts  45.5 us (22%)
  starting transfers between devices  41 us (19%)
  other arithmetic  32.6 us (15%)
  matrix products  31 us (15%)
  blocking collectives  27.8 us (13%)
  waiting for transfers between devices  17.1 us (8%)
  between operations  14.5 us (7%)
    another operation x2, other arithmetic, gla_forward(): cumulative = jnp.cumsum(blocked(logarithm_decay), axis=2)  28.2 us
    all_gather x1, blocking collectives, on_device(): weight_grad = lax.all_gather(summed, 'sp', axis=1, tiled=True)  15.3 us
    all_gather x1, blocking collectives, on_device(): hidden_code_rows = lax.all_gather(compact_factor, 'sp', axis=0, tiled=True)  12.5 us
    unnamed x72, local copies, waits for them, and re-layouts  11.4 us
    dot_general x3, matrix products, carry_states(): return jnp.einsum('hnmk,mhkv->nhkv', weights, increments, precision=highest)  9.75 us
    dot_general x3, matrix products, gla_forward(): jnp.einsum('hnik,hnjk->hnij', query_decayed, key_inverse, precision=highest)  8.16 us
    all_to_all x1, waiting for transfers between devices, on_device(): lax.all_to_all(probe_vectors, 'sp', split_axis=1, concat_axis=0, tiled=True)  7.02 us
    all_to_all x1, starting transfers between devices, on_device(): lax.all_to_all(surplus_damping, 'sp', split_axis=1, concat_axis=0, tiled=...  6.49 us
  transfers between devices with their start and end apart: 12, of which 6 were waited for; matrix products, arithmetic and copies ran while one was open for 31% of the time, Pallas kernels for 0%

profile of v1, /device:TPU:0, one launch (start us, length us, event | category | flops | bytes accessed | tf_op | source)
XLA Modules:
  0.0 209.5 jit_solution(167029506770008685)
XLA Ops:
  7.2 6.5 %all-to-all-start.1 = ((bf16[128,4,4]{0,2,1:T(4,128)(2,1)}), bf16[128,4,4]{0,2,1:T(4,128)(2,1)S(1)}, u32[]{:S(2)}, u32[]{:S(2)}) async-start(bf16[128,4,4]{0,2,1:T(4,128)(2,1)} %bitcast.168), calls=%async_computation.1 | async-start | bytes 8192 | tf_op jit(solution)/shard_map/all_to_all | solution.py:84
  13.7 1.8 copy.214
  15.5 3.8 %all-to-all-done.1 = bf16[128,4,4]{0,2,1:T(4,128)(2,1)S(1)} async-done(((bf16[128,4,4]{0,2,1:T(4,128)(2,1)}), bf16[128,4,4]{0,2,1:T(4,128)(2,1)S(1)}, u32[]{:S(2)}, u32[]{:S(2)}) %all-to-all-start.1) | async-done | bytes 4128 | tf_op jit(solution)/shard_map/all_to_all | solution.py:84
  19.3 3.5 %all-to-all-start.5 = ((bf16[128,4,256]{0,2,1:T(8,128)(2,1)}), bf16[128,4,256]{0,2,1:T(8,128)(2,1)S(1)}, u32[]{:S(2)}, u32[]{:S(2)}) async-start(bf16[128,4,256]{0,2,1:T(8,128)(2,1)} %bitcast.24), calls=%async_computation.5 | async-start | bytes 524288 | tf_op jit(solution)/shard_map/all_to_all | solution.py:80
  23.7 7.0 %all-to-all-done.5 = bf16[128,4,256]{0,2,1:T(8,128)(2,1)S(1)} async-done(((bf16[128,4,256]{0,2,1:T(8,128)(2,1)}), bf16[128,4,256]{0,2,1:T(8,128)(2,1)S(1)}, u32[]{:S(2)}, u32[]{:S(2)}) %all-to-all-start.5) | async-done | bytes 262176 | tf_op jit(solution)/shard_map/all_to_all | solution.py:80
  30.7 3.4 %all-to-all-start = ((bf16[128,4,256]{0,2,1:T(8,128)(2,1)}), bf16[128,4,256]{0,2,1:T(8,128)(2,1)S(1)}, u32[]{:S(2)}, u32[]{:S(2)}) async-start(bf16[128,4,256]{0,2,1:T(8,128)(2,1)} %bitcast), calls=%async_computation | async-start | bytes 524288 | tf_op jit(solution)/shard_map/all_to_all | solution.py:81
  35.7 12.5 %all_gather.6 = bf16[512,64]{0,1:T(8,128)(2,1)S(1)} all-gather(bf16[128,64]{0,1:T(8,128)(2,1)S(1)} %copy-done.31), channel_id=1, replica_groups=mesh['sp'=4,'dp'=8] {'sp'}, dimensions={0}, use_global_device_ids=true | all-gather | bytes 81920 | tf_op jit(solution)/shard_map/all_gather | solution.py:87
  48.8 1.3 fusion.20
  50.8 4.1 %all-to-all-start.3 = ((bf16[128,4,512]{2,0,1:T(8,128)(2,1)}), bf16[128,4,512]{2,0,1:T(8,128)(2,1)}, u32[]{:S(2)}, u32[]{:S(2)}) async-start(bf16[128,4,512]{2,0,1:T(8,128)(2,1)} %bitcast.143), calls=%async_computation.3 | async-start | bytes 1048576 | tf_op jit(solution)/shard_map/all_to_all | solution.py:83
  57.2 25.9 %fusion.46 = f32[4,8,64,64]{3,1,2,0:T(8,128)S(1)} fusion(f32[4,8,64,64]{3,1,2,0:T(8,128)S(1)} %copy.194), kind=kOutput, calls=%fused_computation.84 | output fusion | flops 8257536 | bytes 1048576 | tf_op jit(solution)/shard_map/jvp(jit(cumsum))/reduce_window_sum | solution.py:43
  83.1 5.1 %all-to-all-start.2 = ((bf16[128,4,512]{2,0,1:T(8,128)(2,1)}), bf16[128,4,512]{2,0,1:T(8,128)(2,1)}, u32[]{:S(2)}, u32[]{:S(2)}) async-start(bf16[128,4,512]{2,0,1:T(8,128)(2,1)} %bitcast.144), calls=%async_computation.2 | async-start | bytes 1048576 | tf_op jit(solution)/shard_map/all_to_all | solution.py:82
  93.0 1.2 reshape.166
  94.2 2.0 reshape.161
  96.2 1.9 copy.205
  98.5 2.0 reshape.159
  100.5 1.2 copy.198
  102.8 2.9 %convolution_bitcast_fusion = f32[8,4,64,128]{3,0,2,1:T(8,128)S(1)} fusion(f32[4,64,128,8]{2,1,3,0:T(8,128)S(1)} %convolution_bitcast_fusion.3, f32[4,8,64]{1,2,0:T(8,128)S(1)} %copy-done.23, f32[4,8,64]{1,2,0:T(8,128)S(1)} %copy-done.24, pred[8,8]{1,0:T(8,128)(4,1)S(1)} %copy-done.32), kind=kOutput, calls=%fused_computation.4 | convolution fusion | flops 25214976 | bytes 2113600 | tf_op jit(solution)/shard_map/transpose(jvp(hnmk,mhkv->nhkv))/dot_general | solution.py:32
  105.8 2.8 %fusion.18 = (f32[4,8,64]{2,1,0:T(8,128)}, f32[4,8,64,64]{2,3,1,0:T(8,128)S(1)}, f32[4,8,64,64]{2,3,1,0:T(8,128)}) fusion(f32[4,8,64,64]{2,3,1,0:T(8,128)S(1)} %copy.195, f32[4,8,64,64]{2,1,3,0:T(8,128)S(1)} %reshape.166, f32[4,8,64]{2,1,0:T(8,128)S(1)} %slice_bitcast_fusion, bf16[4,8,64,128]{3,2,1,0:T(8,128)(2,1)S(1)} %bitcast.150, ...), kind=kOutput, calls=%fused_computation.40 | convolution fusion | flops 201979904 | bytes 3686400 | tf_op jit(solution)/shard_map/transpose(jvp(hnjk,hnjv->nhkv))/dot_general | solution.py:55
  109.6 2.5 %convolution_bitcast_fusion.1 = f32[8,4,64,128]{3,0,2,1:T(8,128)S(1)} fusion(f32[8,4,64,128]{3,2,1,0:T(8,128)S(1)} %fusion.6, f32[4,8,64]{1,2,0:T(8,128)S(1)} %copy-done.23, f32[4,8,64]{1,2,0:T(8,128)S(1)} %copy-done.24, pred[8,8]{1,0:T(8,128)(4,1)S(1)} %copy-done.32), kind=kOutput, calls=%fused_computation.6 | convolution fusion | flops 25214976 | bytes 2113600 | tf_op jit(solution)/shard_map/jvp(hnmk,mhkv->nhkv)/dot_general | solution.py:32
  112.1 4.3 %fusion.45 = (f32[4,8,64]{1,2,0:T(8,128)}, f32[4,8,64]{1,2,0:T(8,128)}) fusion(f32[4,8,64]{1,2,0:T(8,128)S(1)} %copy-done.23, f32[4,8,64]{1,2,0:T(8,128)S(1)} %copy-done.24, f32[8,4,64,128]{3,2,1,0:T(8,128)S(1)} %fusion.6, f32[4,64,128,8]{2,1,3,0:T(8,128)S(1)} %convolution_bitcast_fusion.3, pred[8,8]{1,0:T(8,128)(4,1)S(1)} %copy-done.32), kind=kOutput, calls=%fused_computation.83 | convolution fusion | flops 25276416 | bytes 2129984 | tf_op jit(solution)/shard_map/transpose(jvp(hnmk,mhkv->nhkv))/dot_general | solution.py:32
  116.4 2.0 convolution_bitcast_fusion.4
  120.0 1.4 copy.243
  121.4 1.4 copy.244
  122.8 1.4 copy.245
  124.2 1.6 convolution_select_fusion
  125.9 1.3 fusion.44
  127.7 1.5 fusion.3
  129.2 3.7 %pad_add_fusion = (f32[4,8,64,64]{2,3,1,0:T(8,128)}, bf16[4,8,64,64]{2,3,1,0:T(8,128)(2,1)}, bf16[4,8,64,64]{2,3,1,0:T(8,128)(2,1)S(1)}) fusion(f32[4,8,1,64]{2,3,1,0:T(8,128)S(1)} %fusion.3, f32[4,8,64,64]{2,3,1,0:T(8,128)S(1)} %fusion.44, f32[4,8,64,64]{2,1,3,0:T(8,128)S(1)} %mul.72, f32[4,8,64,64]{2,3,1,0:T(8,128)S(1)} %copy.195, ...), kind=kOutput, calls=%fused_computation.22 | convolution fusion | flops 103677952 | bytes 4734976 | tf_op jit(solution)/shard_map/transpose(jvp(hnik,hnjk->hnij))/dot_general | solution.py:50
  133.0 1.1 copy.212
  134.1 1.4 convert_element_type.73
  136.3 1.7 copy.213
  138.0 4.9 %all-to-all-start.4 = ((bf16[4,128,256]{1,2,0:T(8,128)(2,1)}), bf16[4,128,256]{1,2,0:T(8,128)(2,1)S(1)}, u32[]{:S(2)}, u32[]{:S(2)}) async-start(bf16[4,128,256]{1,2,0:T(8,128)(2,1)} %copy.213), calls=%async_computation.4 | async-start | bytes 524288 | tf_op jit(solution)/shard_map/all_to_all | solution.py:110
  142.8 3.1 %convolution_select_fusion.2 = f32[4,8,64,64]{3,2,1,0:T(8,128)} fusion(pred[64,64]{1,0:T(8,128)(4,1)S(1)} %copy-done.28, f32[4,8,64,64]{2,1,3,0:T(8,128)S(1)} %reshape.166, f32[4,8,64,64]{2,3,1,0:T(8,128)S(1)} %copy.195, f32[4,8,64,64]{2,1,3,0:T(8,128)S(1)} %mul.72), kind=kOutput, calls=%fused_computation.11 | convolution fusion | flops 101187584 | bytes 2101248 | tf_op jit(solution)/shard_map/jvp(hnik,hnjk->hnij)/dot_general | solution.py:50
  146.0 2.6 %copy.246 = f32[4,8,64,64]{3,1,2,0:T(8,128)} copy(f32[4,8,64,64]{2,3,1,0:T(8,128)} %get-tuple-element.22) | data formatting | bytes 1048576 | tf_op jit(solution)/shard_map/transpose(jvp())/add_any | solution.py:44
  150.3 1.9 fusion.11
  152.1 5.1 %all-to-all-start.6 = ((bf16[4,128,256]{1,2,0:T(8,128)(2,1)}), bf16[4,128,256]{1,2,0:T(8,128)(2,1)}, u32[]{:S(2)}, u32[]{:S(2)}) async-start(bf16[4,128,256]{1,2,0:T(8,128)(2,1)} %copy.226), calls=%async_computation.6 | async-start | bytes 524288 | tf_op jit(solution)/shard_map/all_to_all | solution.py:113
  157.2 2.3 %fusion.47 = f32[4,8,64,64]{3,1,2,0:T(8,128)S(1)} fusion(f32[4,8,64,64]{3,1,2,0:T(8,128)} %copy.246), kind=kOutput, calls=%fused_computation.85 | output fusion | flops 8257536 | bytes 1048576 | tf_op jit(solution)/shard_map/transpose(jvp(jit(cumsum)))/reduce_window_sum | solution.py:43
  159.5 1.4 copy.247
  160.9 1.6 reshape.163
  165.0 5.2 %all-to-all-start.7 = ((bf16[4,128,512]{2,1,0:T(8,128)(2,1)}), bf16[4,128,512]{2,1,0:T(8,128)(2,1)S(1)}, u32[]{:S(2)}, u32[]{:S(2)}) async-start(bf16[4,128,512]{2,1,0:T(8,128)(2,1)} %convert_element_type.84), calls=%async_computation.7 | async-start | bytes 1048576 | tf_op jit(solution)/shard_map/all_to_all | solution.py:116
  172.6 1.6 collective-permute-start.1
  174.2 2.8 %collective-permute-done.1 = f32[64,256]{1,0:T(8,128)S(1)} collective-permute-done((f32[64,256]{1,0:T(8,128)S(1)}, f32[64,256]{1,0:T(8,128)S(1)}, u32[]{:S(2)}, u32[]{:S(2)}) %collective-permute-start.1) | collective-permute-done | bytes 65568 | tf_op jit(solution)/shard_map/ppermute | solution.py:17
  177.0 1.6 collective-permute-start.2
  178.6 2.7 %collective-permute-done.2 = f32[64,256]{1,0:T(8,128)S(1)} collective-permute-done((f32[64,256]{1,0:T(8,128)S(1)}, f32[64,256]{1,0:T(8,128)S(1)}, u32[]{:S(2)}, u32[]{:S(2)}) %collective-permute-start.2) | collective-permute-done | bytes 65568 | tf_op jit(solution)/shard_map/ppermute | solution.py:17
  181.3 15.3 %all_gather.7 = f32[64,1024]{1,0:T(8,128)S(1)} all-gather(f32[64,256]{1,0:T(8,128)S(1)} %add.52), channel_id=1, replica_groups=mesh['sp'=4,'dp'=8] {'sp'}, dimensions={1}, use_global_device_ids=true | all-gather | bytes 327680 | tf_op jit(solution)/shard_map/all_gather | solution.py:132
  196.6 1.4 convert_element_type.86
  198.9 1.8 copy.249
  200.9 1.0 copy.250
  (122 shorter events, 24.5 us)
Async XLA Ops:
  7.2 41.7 %copy-start = (bf16[64,1024]{1,0:T(8,128)(2,1)S(1)}, bf16[64,1024]{1,0:T(8,128)(2,1)}, u32[]{:S(2)}) copy-start(bf16[64,1024]{1,0:T(8,128)(2,1)} %param.13) | copy-start | bytes 393220
  7.2 12.1 %all-to-all-start.1 = ((bf16[128,4,4]{0,2,1:T(4,128)(2,1)}), bf16[128,4,4]{0,2,1:T(4,128)(2,1)S(1)}, u32[]{:S(2)}, u32[]{:S(2)}) async-start(bf16[128,4,4]{0,2,1:T(4,128)(2,1)} %bitcast.168), calls=%async_computation.1 | async-start | bytes 8192 | tf_op jit(solution)/shard_map/all_to_all | solution.py:84
  19.3 3.6 %copy-start.20 = (bf16[128,1024]{1,0:T(8,128)(2,1)S(1)}, bf16[128,1024]{1,0:T(8,128)(2,1)}, u32[]{:S(2)}) copy-start(bf16[128,1024]{1,0:T(8,128)(2,1)} %param.9) | copy-start | bytes 786436
  19.3 11.4 %all-to-all-start.5 = ((bf16[128,4,256]{0,2,1:T(8,128)(2,1)}), bf16[128,4,256]{0,2,1:T(8,128)(2,1)S(1)}, u32[]{:S(2)}, u32[]{:S(2)}) async-start(bf16[128,4,256]{0,2,1:T(8,128)(2,1)} %bitcast.24), calls=%async_computation.5 | async-start | bytes 524288 | tf_op jit(solution)/shard_map/all_to_all | solution.py:80
  22.8 11.3 %copy-start.17 = (bf16[128,2048]{1,0:T(8,128)(2,1)S(1)}, bf16[128,2048]{1,0:T(8,128)(2,1)}, u32[]{:S(2)}) copy-start(bf16[128,2048]{1,0:T(8,128)(2,1)} %param.11) | copy-start | bytes 1572868
  30.7 19.4 %all-to-all-start = ((bf16[128,4,256]{0,2,1:T(8,128)(2,1)}), bf16[128,4,256]{0,2,1:T(8,128)(2,1)S(1)}, u32[]{:S(2)}, u32[]{:S(2)}) async-start(bf16[128,4,256]{0,2,1:T(8,128)(2,1)} %bitcast), calls=%async_computation | async-start | bytes 524288 | tf_op jit(solution)/shard_map/all_to_all | solution.py:81
  34.1 1.6 copy-start.31
  48.2 1.9 copy-start.21
  50.1 0.7 copy-start.15
  50.1 5.4 %copy-start.18 = (bf16[128,2048]{1,0:T(8,128)(2,1)S(1)}, bf16[128,2048]{1,0:T(8,128)(2,1)}, u32[]{:S(2)}) copy-start(bf16[128,2048]{1,0:T(8,128)(2,1)} %param.10) | copy-start | bytes 1572868
  50.8 32.2 %all-to-all-start.3 = ((bf16[128,4,512]{2,0,1:T(8,128)(2,1)}), bf16[128,4,512]{2,0,1:T(8,128)(2,1)}, u32[]{:S(2)}, u32[]{:S(2)}) async-start(bf16[128,4,512]{2,0,1:T(8,128)(2,1)} %bitcast.143), calls=%async_computation.3 | async-start | bytes 1048576 | tf_op jit(solution)/shard_map/all_to_all | solution.py:83
  83.1 15.5 %all-to-all-start.2 = ((bf16[128,4,512]{2,0,1:T(8,128)(2,1)}), bf16[128,4,512]{2,0,1:T(8,128)(2,1)}, u32[]{:S(2)}, u32[]{:S(2)}) async-start(bf16[128,4,512]{2,0,1:T(8,128)(2,1)} %bitcast.144), calls=%async_computation.2 | async-start | bytes 1048576 | tf_op jit(solution)/shard_map/all_to_all | solution.py:82
  90.6 1.0 copy-start.16
  100.5 1.2 copy-start.1
  101.7 7.0 %copy-start.5 = (bf16[4,512,128]{2,1,0:T(8,128)(2,1)}, bf16[4,512,128]{2,1,0:T(8,128)(2,1)S(1)}, u32[]{:S(2)}) copy-start(bf16[4,512,128]{2,1,0:T(8,128)(2,1)S(1)} %copy.198) | copy-start | bytes 1572868
  101.7 1.1 copy-start.23
  101.7 1.1 copy-start.24
  101.7 1.1 copy-start.32
  105.8 2.9 %copy-start.8 = (f32[8,4,64,128]{3,0,2,1:T(8,128)}, f32[8,4,64,128]{3,0,2,1:T(8,128)S(1)}, u32[]{:S(2)}) copy-start(f32[8,4,64,128]{3,0,2,1:T(8,128)S(1)} %convolution_bitcast_fusion) | copy-start | bytes 3145732
  108.6 1.0 copy-start.3
  116.4 2.0 copy-start.26
  118.4 0.9 copy-start.25
  119.3 0.7 copy-start.30
  121.4 1.4 copy-start.29
  122.8 1.4 copy-start.27
  125.8 1.3 copy-start.11
  125.9 1.5 copy-start.12
  125.9 1.8 copy-start.13
  127.7 1.5 copy-start.7
  127.7 1.5 copy-start.10
  138.0 4.9 %copy-start.28 = (pred[64,64]{1,0:T(8,128)(4,1)S(1)}, pred[64,64]{1,0:T(8,128)(4,1)}, u32[]{:S(2)}) copy-start(pred[64,64]{1,0:T(8,128)(4,1)} %iota_compare_fusion) | copy-start | bytes 12292
  138.0 14.2 %all-to-all-start.4 = ((bf16[4,128,256]{1,2,0:T(8,128)(2,1)}), bf16[4,128,256]{1,2,0:T(8,128)(2,1)S(1)}, u32[]{:S(2)}, u32[]{:S(2)}) async-start(bf16[4,128,256]{1,2,0:T(8,128)(2,1)} %copy.213), calls=%async_computation.4 | async-start | bytes 524288 | tf_op jit(solution)/shard_map/all_to_all | solution.py:110
  146.0 2.7 %copy-start.14 = (bf16[4,8,64,64]{2,3,1,0:T(8,128)(2,1)S(1)}, bf16[4,8,64,64]{2,3,1,0:T(8,128)(2,1)}, u32[]{:S(2)}) copy-start(bf16[4,8,64,64]{2,3,1,0:T(8,128)(2,1)} %get-tuple-element.23) | copy-start | bytes 786436
  148.6 1.5 copy-start.9
  149.0 1.3 copy-start.4
  152.1 12.9 %all-to-all-start.6 = ((bf16[4,128,256]{1,2,0:T(8,128)(2,1)}), bf16[4,128,256]{1,2,0:T(8,128)(2,1)}, u32[]{:S(2)}, u32[]{:S(2)}) async-start(bf16[4,128,256]{1,2,0:T(8,128)(2,1)} %copy.226), calls=%async_computation.6 | async-start | bytes 524288 | tf_op jit(solution)/shard_map/all_to_all | solution.py:113
  160.9 1.6 copy-start.2
  160.9 1.7 copy-start.6
  165.0 5.2 %copy-start.19 = (f32[256,512]{1,0:T(8,128)S(1)}, f32[256,512]{1,0:T(8,128)}, u32[]{:S(2)}) copy-start(f32[256,512]{1,0:T(8,128)} %get-tuple-element.30) | copy-start | bytes 1572868
  165.0 35.6 %all-to-all-start.7 = ((bf16[4,128,512]{2,1,0:T(8,128)(2,1)}), bf16[4,128,512]{2,1,0:T(8,128)(2,1)S(1)}, u32[]{:S(2)}, u32[]{:S(2)}) async-start(bf16[4,128,512]{2,1,0:T(8,128)(2,1)} %convert_element_type.84), calls=%async_computation.7 | async-start | bytes 1048576 | tf_op jit(solution)/shard_map/all_to_all | solution.py:116
  170.3 26.4 %reduce-scatter.2.cloned.1.call-start = ((), (), s32[]{:S(2)}) async-start(), calls=%async_computation.9 | async-start | bytes 163840 | tf_op jit(solution)/shard_map/reduce_scatter | solution.py:125
  170.3 0.8 copy-start.22
  171.3 1.3 collective-permute-start
  172.6 4.3 %collective-permute-start.1 = (f32[64,256]{1,0:T(8,128)S(1)}, f32[64,256]{1,0:T(8,128)S(1)}, u32[]{:S(2)}, u32[]{:S(2)}) collective-permute-start(f32[64,256]{1,0:T(8,128)S(1)} %add.50), channel_id=1, source_target_pairs={{0,2},{1,3},{2,0},{3,1},{4,6},{5,7},{6,4},{7,5},{8,10},{9,11},{10,... | collective-permute-start | bytes 196616 | tf_op jit(solution)/shard_map/ppermute | solution.py:17
  177.0 4.3 %collective-permute-start.2 = (f32[64,256]{1,0:T(8,128)S(1)}, f32[64,256]{1,0:T(8,128)S(1)}, u32[]{:S(2)}, u32[]{:S(2)}) collective-permute-start(f32[64,256]{1,0:T(8,128)S(1)} %add.51), channel_id=1, source_target_pairs={{0,4},{1,5},{2,6},{3,7},{4,0},{5,1},{6,2},{7,3},{8,12},{9,13},{10,... | collective-permute-start | bytes 196616 | tf_op jit(solution)/shard_map/ppermute | solution.py:17
Sparse Core Ops, SparseCore 0:
  173.9 21.1 reduce-scatter.1
